TPU v7x, 32 devices: a whole 2x2x4 slice. The times are simulated.
32 devices in a mesh: sp: 8 (over z, y), dp: 4 (over x, core).
Axes of the slice: x: 2, y: 2, z: 4, core: 2. Of those that a mesh axis runs over, the one named last changes fastest.
Arguments:
- queries: bfloat16 [16, 16, 512, 128], P('dp', None, 'sp'), may hold values from -6 to 6
- key_maps: bfloat16 [16, 16, 512, 128], P('dp', None, 'sp'), may hold values from -6 to 6
- value_rows: bfloat16 [16, 16, 512, 128], P('dp', None, 'sp'), may hold values from -6 to 6
- gate_logits: bfloat16 [512, 16, 2048], P('sp', 'dp'), may hold values from -6 to 6
- mix_lambda: float32 [16], replicated, may hold values from 0.3 to 0.8
- head_gain: float32 [128], replicated, may hold values from 0.1 to 1.9
- out_weight: bfloat16 [2048, 2048], P('sp', 'dp'), may hold values from -0.125 to 0.125
Outputs:
- projected: bfloat16 [512, 16, 2048], P('sp', 'dp')
All inputs are finite; a program needn't handle non-finite values.
Results may differ from a plain program's by a relative error of at most 0.0075.
Values may be sent and summed in bfloat16 or wider, within the bound.
No kernel may reach another device: no remote copies, remote signals or barrier semaphores. Data moves between devices by JAX's collectives and lax.ppermute only.
A program may use at most 64 MiB of HBM per device.

v0:
```python
import jax
import jax.numpy as jnp
from jax import lax
from jax.sharding import PartitionSpec as P

HEAD_DIM = 64
STRETCH = 64
BLOCK = 512


def shortened(shard):
    return jax.tree.map(lambda a: a.astype(jnp.bfloat16) if a.dtype == jnp.float32 else a, shard)


def attend(operands, head_gain):
    query_item, key_item, value_item, weight_two = operands
    length = query_item.shape[0]
    half_cols = query_item.shape[1] // 2
    value_cols = value_item.shape[1]
    block_len = min(BLOCK, length)
    n_blocks = length // block_len
    score_scale = HEAD_DIM ** (-0.5)
    in_segment = jnp.arange(block_len) // STRETCH
    diag_visible = in_segment[None, :] <= in_segment[:, None]

    def query_block(block_index):
        offset = block_index * block_len
        query_rows = lax.dynamic_slice_in_dim(query_item, offset, block_len, 0)

        def update(carry_state, key_block, value_block, visible):
            updated = []
            for which in range(2):
                running, summed, carried = carry_state[which]
                scores = (
                    jnp.dot(
                        query_rows[:, which * half_cols : (which + 1) * half_cols],
                        key_block[:, which * half_cols : (which + 1) * half_cols].T,
                        preferred_element_type=jnp.float32,
                    )
                    * score_scale
                )
                if visible is not None:
                    scores = jnp.where(visible, scores, -1e30)
                highest = jnp.maximum(running, jnp.max(scores, axis=1, keepdims=True))
                rescale = jnp.exp(running - highest)
                weights = jnp.exp(scores - highest)
                summed = summed * rescale + jnp.sum(weights, axis=1, keepdims=True)
                carried = carried * rescale + jnp.dot(
                    weights.astype(jnp.bfloat16), value_block, preferred_element_type=jnp.float32
                )
                updated.append((highest, summed, carried))
            return tuple(updated)

        def advance(key_index, carry_state):
            key_block = lax.dynamic_slice_in_dim(key_item, key_index * block_len, block_len, 0)
            value_block = lax.dynamic_slice_in_dim(value_item, key_index * block_len, block_len, 0)
            return update(carry_state, key_block, value_block, None)

        initial = tuple(
            (
                (
                    jnp.full((block_len, 1), -1e30, jnp.float32),
                    jnp.zeros((block_len, 1), jnp.float32),
                    jnp.zeros((block_len, value_cols), jnp.float32),
                )
                for which in range(2)
            )
        )
        carry_state = lax.fori_loop(0, block_index, advance, initial)
        carry_state = update(
            carry_state,
            lax.dynamic_slice_in_dim(key_item, offset, block_len, 0),
            lax.dynamic_slice_in_dim(value_item, offset, block_len, 0),
            diag_visible,
        )
        combined = carry_state[0][2] / carry_state[0][1] - weight_two * (
            carry_state[1][2] / carry_state[1][1]
        )
        mean_sq = jnp.mean(combined * combined, axis=1, keepdims=True)
        return (combined * lax.rsqrt(mean_sq + 1e-05) * head_gain).astype(jnp.bfloat16)

    pieces = lax.map(query_block, jnp.arange(n_blocks))
    return pieces.reshape(length, value_cols)


def on_device(queries, key_maps, value_rows, gate_logits, mix_lambda, head_gain, out_weight):
    seq_count, head_count, tok_rows, q_cols = queries.shape
    value_cols = value_rows.shape[3]
    item_count = seq_count * head_count
    model_width = gate_logits.shape[2]
    moved = (
        lax.all_to_all(
            queries.reshape(item_count, tok_rows, q_cols),
            "sp",
            split_axis=0,
            concat_axis=1,
            tiled=True,
        ),
        lax.all_to_all(
            key_maps.reshape(item_count, tok_rows, q_cols),
            "sp",
            split_axis=0,
            concat_axis=1,
            tiled=True,
        ),
        lax.all_to_all(
            value_rows.reshape(item_count, tok_rows, value_cols),
            "sp",
            split_axis=0,
            concat_axis=1,
            tiled=True,
        ),
    )
    query_all, key_all, value_all = moved
    per_dev = query_all.shape[0]
    first_item = lax.axis_index("sp") * per_dev
    head_ids = (first_item + jnp.arange(per_dev)) % head_count
    matches = head_ids[:, None] == jnp.arange(head_count)[None, :]
    lambda_local = jnp.sum(jnp.where(matches, mix_lambda[None, :], 0.0), axis=1)

    def attend_one(operands):
        return attend(operands, head_gain)

    normed = lax.map(attend_one, (query_all, key_all, value_all, lambda_local))
    returned = lax.all_to_all(
        shortened(jnp.swapaxes(normed, 0, 1)), "sp", split_axis=0, concat_axis=1, tiled=True
    )
    by_token = returned.reshape(tok_rows, seq_count, model_width)
    gated = (jax.nn.sigmoid(gate_logits.astype(jnp.float32)) * by_token.astype(jnp.float32)).astype(
        jnp.bfloat16
    )
    gated_rows = gated.reshape(tok_rows * seq_count, model_width)
    gathered = lax.all_gather(out_weight, "sp", axis=0, tiled=True)
    result = jnp.dot(
        gated_rows,
        lax.all_gather(gathered, "dp", axis=1, tiled=True),
        preferred_element_type=jnp.float32,
    )
    return result.astype(jnp.bfloat16).reshape(tok_rows, seq_count, model_width)


def solution(mesh):
    placed = (
        P("dp", None, "sp", None),
        P("dp", None, "sp", None),
        P("dp", None, "sp", None),
        P("sp", "dp", None),
        P(),
        P(),
        P("sp", "dp"),
    )
    return jax.shard_map(
        on_device, mesh=mesh, in_specs=placed, out_specs=P("sp", "dp", None), check_vma=False
    )
```

profile of v0, /device:TPU:0, one launch (start us, length us, event | category | flops | bytes accessed | tf_op | source)
XLA Modules:
  0.0 221.4 jit_solution(4606228928445615071)
XLA Ops:
  6.5 33.1 %all_to_all.63 = bf16[64,64,128]{2,1,0:T(8,128)(2,1)S(1)} all-to-all(bf16[64,64,128]{2,1,0:T(8,128)(2,1)} %bitcast.57), channel_id=1, replica_groups=mesh['sp'=8,'dp'=4] {'sp'}, dimensions={0} | all-to-all | bytes 2097152 | tf_op jit(solution)/shard_map/all_to_all | solution.py:99
  39.6 3.7 %all-to-all-start.2 = ((bf16[64,64,128]{2,1,0:T(8,128)(2,1)}), bf16[64,64,128]{2,1,0:T(8,128)(2,1)S(1)}, u32[]{:S(2)}, u32[]{:S(2)}) async-start(bf16[64,64,128]{2,1,0:T(8,128)(2,1)} %bitcast.13), calls=%async_computation.2 | async-start | bytes 2097152 | tf_op jit(solution)/shard_map/all_to_all | solution.py:106
  43.4 0.7 all-gather.3.cloned.1.call-update
  44.1 33.3 %all-to-all-done.2 = bf16[64,64,128]{2,1,0:T(8,128)(2,1)S(1)} async-done(((bf16[64,64,128]{2,1,0:T(8,128)(2,1)}), bf16[64,64,128]{2,1,0:T(8,128)(2,1)S(1)}, u32[]{:S(2)}, u32[]{:S(2)}) %all-to-all-start.2) | async-done | bytes 1048608 | tf_op jit(solution)/shard_map/all_to_all | solution.py:106
  77.3 3.6 %all-to-all-start = ((bf16[64,64,128]{2,1,0:T(8,128)(2,1)}), bf16[64,64,128]{2,1,0:T(8,128)(2,1)S(1)}, u32[]{:S(2)}, u32[]{:S(2)}) async-start(bf16[64,64,128]{2,1,0:T(8,128)(2,1)} %bitcast.58), calls=%async_computation | async-start | bytes 2097152 | tf_op jit(solution)/shard_map/all_to_all | solution.py:92
  81.2 1.1 copy.16
  82.2 1.1 copy.17
  83.3 40.0 %all-to-all-done = bf16[64,64,128]{2,1,0:T(8,128)(2,1)S(1)} async-done(((bf16[64,64,128]{2,1,0:T(8,128)(2,1)}), bf16[64,64,128]{2,1,0:T(8,128)(2,1)S(1)}, u32[]{:S(2)}, u32[]{:S(2)}) %all-to-all-start) | async-done | bytes 1048608 | tf_op jit(solution)/shard_map/all_to_all | solution.py:92
  123.4 1.1 copy-done
  124.5 47.8 %while.86 = (s32[]{:T(128)}, bf16[8,512,128]{1,2,0:T(8,128)(2,1)S(1)}, bf16[8,512,128]{2,1,0:T(8,128)(2,1)S(1)}, bf16[8,512,128]{2,1,0:T(8,128)(2,1)}, bf16[8,51...) while((s32[]{:T(128)}, bf16[8,512,128]{1,2,0:T(8,128)(2,1)S(1)}, ...), condition=%wide.region_7.8_spmd, body=%wide.region_1.7_spmd.sunk | while | flops 206249472 | bytes 8851561 | solution.py:124
  124.5 0.9 dynamic-slice_bitcast_fusion.3
  126.6 1.2 fusion.49
  127.9 0.6 dynamic_slice.56
  128.4 1.9 multiply_reduce_fusion.2
  130.5 1.0 dynamic-slice_bitcast_fusion.3
  132.6 1.3 fusion.49
  133.9 0.6 dynamic_slice.56
  134.5 1.9 multiply_reduce_fusion.2
  136.6 0.9 dynamic-slice_bitcast_fusion.3
  138.7 1.2 fusion.49
  139.9 0.6 dynamic_slice.56
  140.5 1.9 multiply_reduce_fusion.2
  142.5 0.9 dynamic-slice_bitcast_fusion.3
  144.6 1.2 fusion.49
  145.9 0.6 dynamic_slice.56
  146.5 1.9 multiply_reduce_fusion.2
  148.5 0.9 dynamic-slice_bitcast_fusion.3
  150.6 1.2 fusion.49
  151.8 0.6 dynamic_slice.56
  152.4 1.9 multiply_reduce_fusion.2
  154.4 0.9 dynamic-slice_bitcast_fusion.3
  156.5 1.2 fusion.49
  157.8 0.6 dynamic_slice.56
  158.4 1.9 multiply_reduce_fusion.2
  160.4 0.9 dynamic-slice_bitcast_fusion.3
  162.5 1.2 fusion.49
  163.7 0.6 dynamic_slice.56
  164.3 1.9 multiply_reduce_fusion.2
  166.4 0.9 dynamic-slice_bitcast_fusion.3
  168.5 1.2 fusion.49
  169.7 0.6 dynamic_slice.56
  170.3 1.9 multiply_reduce_fusion.2
  172.3 0.8 copy.18
  173.1 29.4 %all_to_all.64 = bf16[512,8,128]{2,1,0:T(8,128)(2,1)S(1)} all-to-all(bf16[512,8,128]{2,1,0:T(8,128)(2,1)S(1)} %bitcast.54), channel_id=1, replica_groups=mesh['sp'=8,'dp'=4] {'sp'}, dimensions={0} | all-to-all | bytes 2097152 | tf_op jit(solution)/shard_map/all_to_all | solution.py:125
  202.9 1.7 reshape.107
  204.6 2.7 %fusion.31 = bf16[64,4,2048]{2,1,0:T(4,128)(2,1)S(1)} fusion(f32[64,4,2048]{2,1,0:T(4,128)} %reshape.107, bf16[64,4,2048]{2,1,0:T(4,128)(2,1)S(1)} %copy-done.1), kind=kLoop, calls=%fused_computation.51 | loop fusion | flops 3145728 | bytes 4194304 | tf_op jit(solution)/shard_map/convert_element_type | solution.py:129
  207.6 5.7 %convolution_convert_fusion = bf16[256,2048]{1,0:T(8,128)(2,1)S(1)} fusion(bf16[256,2048]{1,0:T(8,128)(2,1)S(1)} %reshape.103, bf16[2048,2048]{1,0:T(8,128)(2,1)} %all-gather.5.cloned.1.call-done), kind=kOutput, calls=%fused_computation.48 | convolution fusion | flops 2148007936 | bytes 10485760 | tf_op jit(solution)/shard_map/dot_general | solution.py:134
  213.4 1.2 reshape.104
  (107 shorter events, 11.0 us)
Async XLA Ops:
  39.6 41.4 %copy-start.3 = (f32[16]{0:T(128)S(1)}, f32[16]{0:T(128)}, u32[]{:S(2)}) copy-start(f32[16]{0:T(128)} %param.13) | copy-start | bytes 196
  39.6 37.7 %all-to-all-start.2 = ((bf16[64,64,128]{2,1,0:T(8,128)(2,1)}), bf16[64,64,128]{2,1,0:T(8,128)(2,1)S(1)}, u32[]{:S(2)}, u32[]{:S(2)}) async-start(bf16[64,64,128]{2,1,0:T(8,128)(2,1)} %bitcast.13), calls=%async_computation.2 | async-start | bytes 2097152 | tf_op jit(solution)/shard_map/all_to_all | solution.py:106
  43.3 80.1 %all-gather.3.cloned.1.call-start = ((), (), s32[]{:S(2)}) async-start(), calls=%async_computation.4 | async-start | bytes 2359296 | tf_op jit(solution)/shard_map/all_gather | solution.py:133
  77.3 46.0 %all-to-all-start = ((bf16[64,64,128]{2,1,0:T(8,128)(2,1)}), bf16[64,64,128]{2,1,0:T(8,128)(2,1)S(1)}, u32[]{:S(2)}, u32[]{:S(2)}) async-start(bf16[64,64,128]{2,1,0:T(8,128)(2,1)} %bitcast.58), calls=%async_computation | async-start | bytes 2097152 | tf_op jit(solution)/shard_map/all_to_all | solution.py:92
  80.9 126.7 %all-gather.5.cloned.1.call-start = ((), (), s32[]{:S(2)}) async-start(), calls=%async_computation.5 | async-start | bytes 10485760 | tf_op jit(solution)/shard_map/all_gather | solution.py:136
  123.3 1.2 copy-start
  123.3 1.2 copy-start.2
  202.9 1.7 copy-start.1
Sparse Core Ops, SparseCore 0:
  46.3 75.0 all-gather.2
  123.6 57.2 all-gather.4
where the time goes:
time: 222 us; the launch traced here: 221 us
  waiting for transfers between devices  74 us (33%)
  blocking collectives  62.5 us (28%)
  matrix products  36.6 us (16%)
  local copies, waits for them, and re-layouts  19.7 us (9%)
  between operations  13.5 us (6%)
  starting transfers between devices  7.36 us (3%)
  other arithmetic  7.2 us (3%)
    all_to_all x1, waiting for transfers between devices, on_device(): lax.all_to_all(queries.reshape(item_count, tok_rows, q_cols), 'sp', split...  40 us
    all_to_all x1, waiting for transfers between devices, on_device(): lax.all_to_all(value_rows.reshape(item_count, tok_rows, value_cols), 'sp'...  33.3 us
    all_to_all x1, blocking collectives, on_device(): lax.all_to_all(key_maps.reshape(item_count, tok_rows, q_cols), 'sp', spli...  33.1 us
    all_to_all x1, blocking collectives, on_device(): lax.all_to_all(shortened(jnp.swapaxes(normed, 0, 1)), 'sp', split_axis=0,...  29.4 us
    dot_general x16, matrix products, update(): jnp.dot(weights.astype(jnp.bfloat16), value_block, preferred_element_type...  25.1 us
    squeeze x8, local copies, waits for them, and re-layouts, on_device(): normed = lax.map(attend_one, (query_all, key_all, value_all, lambda_local))  7.44 us
    dot_general x16, matrix products, update(): jnp.dot(query_rows[:, which * half_cols:(which + 1) * half_cols], key_blo...  5.72 us
    dot_general x1, matrix products, on_device(): jnp.dot(gated_rows, lax.all_gather(gathered, 'dp', axis=1, tiled=True), p...  5.71 us
  transfers between devices with their start and end apart: 4, of which 2 were waited for; matrix products, arithmetic and copies ran while one was open for 25% of the time, Pallas kernels for 0%

commit v1 on v0

v1 whole, which is shorter than its diff:
```python
import functools
import math

import jax
import jax.numpy as jnp
from jax import lax
from jax.experimental import pallas as pl
from jax.experimental.pallas import tpu as pltpu
from jax.sharding import PartitionSpec as P

STRETCH = 64
EPS = 1e-05
HIDDEN = -1e30
LOG2E = math.log2(math.e)


def contract_last(a, b):
    return lax.dot_general(a, b, (((1,), (1,)), ((), ())), preferred_element_type=jnp.float32)


def attend_kernel(place_ref, lam_ref, gain_ref, got_ref, out_ref):
    ranks, _, _, rows, cols = got_ref.shape
    length = ranks * rows
    half = cols // 2
    block = min(length, max(2 * STRETCH, length // 4))
    item = place_ref[0] * pl.num_programs(0) + pl.program_id(0)
    lam = lam_ref[lax.rem(item, lam_ref.shape[0])]
    gain = gain_ref[...]
    query = got_ref[:, 0, 0].reshape(length, cols)
    keys = got_ref[:, 0, 1].reshape(length, cols)
    values = got_ref[:, 0, 2].reshape(length, cols)
    values = jnp.concatenate([values, jnp.ones_like(values)], axis=1)
    first_map = lax.broadcasted_iota(jnp.int32, (block, cols), 1) < half
    row = lax.rem(lax.broadcasted_iota(jnp.int32, (2 * block, block), 0), block)
    col = lax.broadcasted_iota(jnp.int32, (2 * block, block), 1)
    visible = col // STRETCH <= row // STRETCH
    factor = LOG2E * half**-0.5
    for start in range(0, length, block):
        stop = start + block
        part = query[start:stop]
        zero = jnp.zeros_like(part)
        both = jnp.concatenate([jnp.where(first_map, part, zero), jnp.where(first_map, zero, part)], axis=0)
        near = jnp.where(visible, contract_last(both, keys[start:stop]), HIDDEN)
        top = jnp.max(near, axis=1, keepdims=True)
        if start:
            far = contract_last(both, keys[:start])
            top = jnp.maximum(top, jnp.max(far, axis=1, keepdims=True))
        mapped = jnp.dot(
            jnp.exp2((near - top) * factor).astype(jnp.bfloat16),
            values[start:stop],
            preferred_element_type=jnp.float32,
        )
        if start:
            mapped += jnp.dot(
                jnp.exp2((far - top) * factor).astype(jnp.bfloat16),
                values[:start],
                preferred_element_type=jnp.float32,
            )
        mapped = mapped[:, :cols] / mapped[:, cols:]
        combined = mapped[:block] - lam * mapped[block:]
        mean_sq = jnp.mean(combined * combined, axis=1, keepdims=True)
        normed = (combined * lax.rsqrt(mean_sq + EPS) * gain).astype(jnp.bfloat16)
        out_ref[start // rows : stop // rows, 0] = normed.reshape(block // rows, rows, cols)


def attend(got, mix_lambda, head_gain):
    ranks, items, _, rows, cols = got.shape
    place = lax.axis_index("sp").astype(jnp.int32)[None]
    return pl.pallas_call(
        attend_kernel,
        grid=(items,),
        out_shape=jax.ShapeDtypeStruct((ranks, items, rows, cols), jnp.bfloat16),
        in_specs=[
            pl.BlockSpec(memory_space=pltpu.SMEM),
            pl.BlockSpec(memory_space=pltpu.SMEM),
            pl.BlockSpec((1, cols), lambda i: (0, 0)),
            pl.BlockSpec((ranks, 1, 3, rows, cols), lambda i: (0, i, 0, 0, 0)),
        ],
        out_specs=pl.BlockSpec((ranks, 1, rows, cols), lambda i: (0, i, 0, 0)),
        cost_estimate=pl.CostEstimate(flops=6_000_000_000, bytes_accessed=4_000_000, transcendentals=0),
        name="attend",
    )(place, mix_lambda, head_gain[None, :], got)


def project_kernel(normed_ref, gate_ref, weight_ref, out_ref, gated_ref):
    seqs, heads, rows, cols = normed_ref.shape
    total = seqs * rows

    @pl.when(pl.program_id(0) == 0)
    def _():
        to = lax.broadcasted_iota(jnp.int32, (total, total), 0)
        of = lax.broadcasted_iota(jnp.int32, (total, total), 1)
        spread = (of == lax.rem(to, seqs) * rows + to // seqs).astype(jnp.bfloat16)
        for head in range(heads):
            span = slice(head * cols, (head + 1) * cols)
            by_seq = normed_ref[:, head].reshape(total, cols)
            by_token = jnp.dot(spread, by_seq, preferred_element_type=jnp.float32)
            gate = jax.nn.sigmoid(gate_ref[:, span].astype(jnp.float32))
            gated_ref[:, span] = (gate * by_token).astype(jnp.bfloat16)

    out_ref[...] = jnp.dot(gated_ref[...], weight_ref[0], preferred_element_type=jnp.float32).astype(jnp.bfloat16)


def project(normed, gate, weight):
    seqs, heads, rows, cols = normed.shape
    parts, depth, width = weight.shape
    total = seqs * rows
    return pl.pallas_call(
        project_kernel,
        grid=(parts,),
        out_shape=jax.ShapeDtypeStruct((total, parts * width), jnp.bfloat16),
        in_specs=[
            pl.BlockSpec((seqs, heads, rows, cols), lambda j: (0, 0, 0, 0)),
            pl.BlockSpec((total, depth), lambda j: (0, 0)),
            pl.BlockSpec((1, depth, width), lambda j: (j, 0, 0)),
        ],
        out_specs=pl.BlockSpec((total, width), lambda j: (0, j)),
        scratch_shapes=[pltpu.VMEM((total, depth), jnp.bfloat16)],
        cost_estimate=pl.CostEstimate(flops=2_000_000_000, bytes_accessed=10_000_000, transcendentals=0),
        name="project",
    )(normed, gate, weight)


def on_device(queries, key_maps, value_rows, gate_logits, mix_lambda, head_gain, out_weight):
    seqs, heads, rows, cols = queries.shape
    ranks = lax.axis_size("sp")
    items = seqs * heads // ranks
    width = gate_logits.shape[2]
    sent = jnp.stack([a.reshape(ranks, items, rows, cols) for a in (queries, key_maps, value_rows)], axis=2)
    got = lax.all_to_all(sent, "sp", split_axis=0, concat_axis=0, tiled=True)
    normed = attend(got, mix_lambda, head_gain)
    returned = lax.all_to_all(normed, "sp", split_axis=0, concat_axis=0, tiled=True)
    weight = lax.all_gather(out_weight, "sp", axis=0, tiled=True)
    weight = lax.all_gather(weight, "dp", axis=0, tiled=False)
    result = project(
        returned.reshape(seqs, heads, rows, cols), gate_logits.reshape(rows * seqs, width), weight
    )
    return result.reshape(rows, seqs, width)


def solution(mesh):
    placed = (
        P("dp", None, "sp", None),
        P("dp", None, "sp", None),
        P("dp", None, "sp", None),
        P("sp", "dp", None),
        P(),
        P(),
        P("sp", "dp"),
    )
    return jax.shard_map(
        on_device, mesh=mesh, in_specs=placed, out_specs=P("sp", "dp", None), check_vma=False
    )
```

time: 222 us -> 201 us (0.905)
  waiting for transfers between devices: 74 us -> 148 us
  blocking collectives: 62.5 us -> 0 us
  matrix products: 36.6 us -> 0 us
  Pallas kernels: 0 us -> 21.1 us
  local copies, waits for them, and re-layouts: 19.7 us -> 7.14 us
  other arithmetic: 7.2 us -> 3.9 us
    all_to_all x2 -> x0, blocking collectives: 62.5 us -> none  [the longest x1 33.1 us: on_device(): lax.all_to_all(key_maps.reshape(item_count, tok_rows, q_cols), 'sp', spli...]
    all_gather x2, waiting for transfers between devices: 0.04 us -> 54 us  [the longest x1 54 us: on_device(): weight = lax.all_gather(out_weight, 'sp', axis=0, tiled=True)]
    dot_general x33 -> x0, matrix products: 36.6 us -> none  [the longest x16 25.1 us: update(): jnp.dot(weights.astype(jnp.bfloat16), value_block, preferred_element_type...]
    pallas_call x0 -> x2, Pallas kernels: none -> 21.1 us  [the longest x1 13.5 us: attend(): pl.pallas_call(attend_kernel, grid=(items,), out_shape=jax.ShapeDtypeStru...]
    all_to_all x2, waiting for transfers between devices: 73.2 us -> 93.3 us  [the longest x1 69.6 us: on_device(): got = lax.all_to_all(sent, 'sp', split_axis=0, concat_axis=0, tiled=True)]
    squeeze x8 -> x0, local copies, waits for them, and re-layouts: 7.44 us -> none  [on_device(): normed = lax.map(attend_one, (query_all, key_all, value_all, lambda_local))]
    dynamic_slice x8 -> x0, local copies, waits for them, and re-layouts: 4.71 us -> none  [on_device(): normed = lax.map(attend_one, (query_all, key_all, value_all, lambda_local))]
    another operation x0 -> x1, other arithmetic: none -> 3.9 us  [on_device(): jnp.stack([a.reshape(ranks, items, rows, cols) for a in (queries, key_map...]
  transfers between devices with their start and end apart: 4 -> 4, of which waited for: 2 -> 3; matrix products, arithmetic and copies ran while one was open for 25% -> 3% of each run, Pallas kernels for 0% -> 7%
where the time goes in v1:
time: 201 us
  waiting for transfers between devices  148 us (74%)
  Pallas kernels  21.1 us (10%)
  between operations  13.4 us (7%)
  starting transfers between devices  7.37 us (4%)
  local copies, waits for them, and re-layouts  7.14 us (4%)
  other arithmetic  3.9 us (2%)
    all_to_all x1, waiting for transfers between devices, on_device(): got = lax.all_to_all(sent, 'sp', split_axis=0, concat_axis=0, tiled=True)  69.6 us
    all_gather x1, waiting for transfers between devices, on_device(): weight = lax.all_gather(out_weight, 'sp', axis=0, tiled=True)  54 us
    all_to_all x1, waiting for transfers between devices, on_device(): lax.all_to_all(normed, 'sp', split_axis=0, concat_axis=0, tiled=True)  23.7 us
    pallas_call x1, Pallas kernels, attend(): pl.pallas_call(attend_kernel, grid=(items,), out_shape=jax.ShapeDtypeStru...  13.5 us
    pallas_call x1, Pallas kernels, project(): pl.pallas_call(project_kernel, grid=(parts,), out_shape=jax.ShapeDtypeStr...  7.61 us
  transfers between devices with their start and end apart: 4, of which 3 were waited for; matrix products, arithmetic and copies ran while one was open for 3% of the time, Pallas kernels for 7%

profile of v1, /device:TPU:0, one launch (start us, length us, event | category | flops | bytes accessed | tf_op | source)
XLA Modules:
  0.0 201.0 jit_solution(15402059327528869813)
XLA Ops:
  6.5 0.0 all-gather.4.cloned.1.call-start
  6.5 0.7 all-gather.4.cloned.1.call-update
  7.3 0.0 all-gather.6.cloned.1.call-start
  7.3 54.0 %all-gather.4.cloned.1.call-done = bf16[2048,512]{1,0:T(8,128)(2,1)} async-done(((bf16[256,512]{1,0:T(8,128)(2,1)}), bf16[2048,512]{1,0:T(8,128)(2,1)}) %all-gather.4.cloned.1.call-update) | async-done | bytes 2097168 | tf_op jit(solution)/shard_map/all_gather | solution.py:133
  61.3 0.0 all-gather.6.cloned.1.call-update
  61.3 3.9 %pad_maximum_fusion = bf16[8,8,3,64,128]{4,3,2,1,0:T(8,128)(2,1)} fusion(bf16[8,8,1,64,128]{4,3,2,1,0:T(8,128)(2,1)} %bitcast.9, bf16[8,8,1,64,128]{4,3,2,1,0:T(8,128)(2,1)} %bitcast.10, bf16[8,8,1,64,128]{4,3,2,1,0:T(8,128)(2,1)} %bitcast.11), kind=kLoop, calls=%fused_computation | loop fusion | flops 3145728 | bytes 6291456 | tf_op jit(solution)/shard_map/stack | solution.py:129
  65.2 3.7 %all-to-all-start = ((bf16[8,8,3,64,128]{4,3,2,1,0:T(8,128)(2,1)}), bf16[8,8,3,64,128]{4,3,2,1,0:T(8,128)(2,1)S(1)}, u32[]{:S(2)}, u32[]{:S(2)}) async-start(bf16[8,8,3,64,128]{4,3,2,1,0:T(8,128)(2,1)} %pad_maximum_fusion), calls=%async_computation | async-start | bytes 6291456 | tf_op jit(solution)/shard_map/all_to_all | solution.py:130
  68.9 69.6 %all-to-all-done.got_ref = bf16[8,8,3,64,128]{4,3,2,1,0:T(8,128)(2,1)S(1)} async-done(((bf16[8,8,3,64,128]{4,3,2,1,0:T(8,128)(2,1)}), bf16[8,8,3,64,128]{4,3,2,1,0:T(8,128)(2,1)S(1)}, u32[]{:S(2)}, u32[]{:S(2)}) %all-to-all-start) | async-done | bytes 3145760 | tf_op jit(solution)/shard_map/all_to_all | solution.py:130
  138.5 0.0 copy-start.1
  138.5 1.7 copy-done.1
  140.2 13.5 %attend.1 = bf16[8,8,64,128]{3,2,1,0:T(8,128)(2,1)} custom-call(s32[1]{0:T(128)} %bitcast.place_ref, f32[16]{0:T(128)} %lam_ref.1, f32[1,128]{1,0:T(1,128)} %bitcast.12, bf16[8,8,3,64,128]{4,3,2,1,0:T(8,128)(2,1)} %copy-done.1), custom_call_target="tpu_custom_call" | custom-call | flops 6000000000 | bytes 4000000 | tf_op jit(solution)/shard_map/attend/pallas_call | solution.py:69
  153.7 3.6 %all-to-all-start.1 = ((bf16[8,8,64,128]{3,2,1,0:T(8,128)(2,1)}), bf16[8,8,64,128]{3,2,1,0:T(8,128)(2,1)S(1)}, u32[]{:S(2)}, u32[]{:S(2)}) async-start(bf16[8,8,64,128]{3,2,1,0:T(8,128)(2,1)} %attend.1), calls=%async_computation.1 | async-start | bytes 2097152 | tf_op jit(solution)/shard_map/all_to_all | solution.py:132
  157.4 2.2 %reshape.10.gate_ref = bf16[256,2048]{1,0:T(8,128)(2,1)} reshape(bf16[64,4,2048]{2,1,0:T(4,128)(2,1)} %param.10) | data formatting | bytes 2097152 | tf_op jit(solution)/shard_map/reshape | solution.py:136
  159.6 23.7 %all-to-all-done.1 = bf16[8,8,64,128]{3,2,1,0:T(8,128)(2,1)S(1)} async-done(((bf16[8,8,64,128]{3,2,1,0:T(8,128)(2,1)}), bf16[8,8,64,128]{3,2,1,0:T(8,128)(2,1)S(1)}, u32[]{:S(2)}, u32[]{:S(2)}) %all-to-all-start.1) | async-done | bytes 1048608 | tf_op jit(solution)/shard_map/all_to_all | solution.py:132
  183.3 0.0 copy-start
  183.3 0.0 all-gather.6.cloned.1.call-done
  183.3 1.0 copy-done
  184.3 7.6 %project.1 = bf16[256,2048]{1,0:T(8,128)(2,1)} custom-call(bf16[4,16,64,128]{3,2,1,0:T(8,128)(2,1)} %bitcast.8, bf16[256,2048]{1,0:T(8,128)(2,1)} %reshape.10.gate_ref, bf16[4,2048,512]{2,1,0:T(8,128)(2,1)} %bitcast.7), custom_call_target="tpu_custom_call" | custom-call | flops 2000000000 | bytes 10000000 | tf_op jit(solution)/shard_map/project/pallas_call | solution.py:108
  191.9 2.2 %reshape.11 = bf16[64,4,2048]{2,1,0:T(4,128)(2,1)} reshape(bf16[256,2048]{1,0:T(8,128)(2,1)} %project.1) | data formatting | bytes 2097152 | tf_op jit(solution)/shard_map/reshape | solution.py:138
Async XLA Ops:
  6.5 54.8 %all-gather.4.cloned.1.call-start = ((), (), s32[]{:S(2)}) async-start(), calls=%async_computation.2 | async-start | bytes 2359296 | tf_op jit(solution)/shard_map/all_gather | solution.py:133
  7.3 176.1 %all-gather.6.cloned.1.call-start = ((), (), s32[]{:S(2)}) async-start(), calls=%async_computation.3 | async-start | bytes 10485760 | tf_op jit(solution)/shard_map/all_gather | solution.py:134
  65.2 73.3 %all-to-all-start = ((bf16[8,8,3,64,128]{4,3,2,1,0:T(8,128)(2,1)}), bf16[8,8,3,64,128]{4,3,2,1,0:T(8,128)(2,1)S(1)}, u32[]{:S(2)}, u32[]{:S(2)}) async-start(bf16[8,8,3,64,128]{4,3,2,1,0:T(8,128)(2,1)} %pad_maximum_fusion), calls=%async_computation | async-start | bytes 6291456 | tf_op jit(solution)/shard_map/all_to_all | solution.py:130
  138.5 1.7 copy-start.1
  153.7 29.6 %all-to-all-start.1 = ((bf16[8,8,64,128]{3,2,1,0:T(8,128)(2,1)}), bf16[8,8,64,128]{3,2,1,0:T(8,128)(2,1)S(1)}, u32[]{:S(2)}, u32[]{:S(2)}) async-start(bf16[8,8,64,128]{3,2,1,0:T(8,128)(2,1)} %attend.1), calls=%async_computation.1 | async-start | bytes 2097152 | tf_op jit(solution)/shard_map/all_to_all | solution.py:132
  183.3 1.0 copy-start
Sparse Core Ops, SparseCore 0:
  9.5 51.7 all-gather.3
  62.9 56.7 all-gather.5

commit v2 on v1

--- a/solution.py
+++ b/solution.py
@@ -82,43 +82,64 @@
     )(place, mix_lambda, head_gain[None, :], got)
 
 
-def project_kernel(normed_ref, gate_ref, weight_ref, out_ref, gated_ref):
+def project_kernel(place_ref, normed_ref, gate_ref, *refs):
+    weight_refs, out_ref, gated_ref = refs[:-2], refs[-2], refs[-1]
     seqs, heads, rows, cols = normed_ref.shape
     total = seqs * rows
-
-    @pl.when(pl.program_id(0) == 0)
-    def _():
-        to = lax.broadcasted_iota(jnp.int32, (total, total), 0)
-        of = lax.broadcasted_iota(jnp.int32, (total, total), 1)
-        spread = (of == lax.rem(to, seqs) * rows + to // seqs).astype(jnp.bfloat16)
-        for head in range(heads):
-            span = slice(head * cols, (head + 1) * cols)
-            by_seq = normed_ref[:, head].reshape(total, cols)
-            by_token = jnp.dot(spread, by_seq, preferred_element_type=jnp.float32)
-            gate = jax.nn.sigmoid(gate_ref[:, span].astype(jnp.float32))
-            gated_ref[:, span] = (gate * by_token).astype(jnp.bfloat16)
-
-    out_ref[...] = jnp.dot(gated_ref[...], weight_ref[0], preferred_element_type=jnp.float32).astype(jnp.bfloat16)
+    to = lax.broadcasted_iota(jnp.int32, (total, total), 0)
+    of = lax.broadcasted_iota(jnp.int32, (total, total), 1)
+    spread = (of == lax.rem(to, seqs) * rows + to // seqs).astype(jnp.bfloat16)
+    for head in range(heads):
+        span = slice(head * cols, (head + 1) * cols)
+        by_seq = normed_ref[:, head].reshape(total, cols)
+        by_token = jnp.dot(spread, by_seq, preferred_element_type=jnp.float32)
+        gate = jax.nn.sigmoid(gate_ref[:, span].astype(jnp.float32))
+        gated_ref[:, span] = (gate * by_token).astype(jnp.bfloat16)
+    for piece, weight_ref in enumerate(weight_refs):
+        width = weight_ref.shape[1]
+        start = pl.multiple_of(jnp.bitwise_xor(place_ref[0], piece) * width, width)
+        out_ref[:, pl.ds(start, width)] = jnp.dot(
+            gated_ref[...], weight_ref[...], preferred_element_type=jnp.float32
+        ).astype(jnp.bfloat16)
 
 
-def project(normed, gate, weight):
+def project(normed, gate, pieces):
     seqs, heads, rows, cols = normed.shape
-    parts, depth, width = weight.shape
+    depth, width = pieces[0].shape
     total = seqs * rows
+    vmem = pl.BlockSpec(memory_space=pltpu.VMEM)
     return pl.pallas_call(
         project_kernel,
-        grid=(parts,),
-        out_shape=jax.ShapeDtypeStruct((total, parts * width), jnp.bfloat16),
-        in_specs=[
-            pl.BlockSpec((seqs, heads, rows, cols), lambda j: (0, 0, 0, 0)),
-            pl.BlockSpec((total, depth), lambda j: (0, 0)),
-            pl.BlockSpec((1, depth, width), lambda j: (j, 0, 0)),
-        ],
-        out_specs=pl.BlockSpec((total, width), lambda j: (0, j)),
+        out_shape=jax.ShapeDtypeStruct((total, len(pieces) * width), jnp.bfloat16),
+        in_specs=[pl.BlockSpec(memory_space=pltpu.SMEM)] + [vmem] * (2 + len(pieces)),
+        out_specs=vmem,
         scratch_shapes=[pltpu.VMEM((total, depth), jnp.bfloat16)],
         cost_estimate=pl.CostEstimate(flops=2_000_000_000, bytes_accessed=10_000_000, transcendentals=0),
         name="project",
-    )(normed, gate, weight)
+    )(lax.axis_index("dp").astype(jnp.int32)[None], normed, gate, *pieces)
+
+
+def swap(array, axis, bit):
+    return lax.ppermute(array, axis, [(i, i ^ bit) for i in range(lax.axis_size(axis))])
+
+
+def gather_weight(block):
+    ranks, parts = lax.axis_size("sp"), lax.axis_size("dp")
+    me = lax.axis_index("sp")
+    depth, width = block.shape
+    held = block
+    bits = ranks.bit_length() - 1
+    for k in reversed(range(bits)):
+        came = swap(held, "sp", 1 << k)
+        upper = (me >> k) & 1 == 1
+        held = jnp.stack([jnp.where(upper, came, held), jnp.where(upper, held, came)])
+    held = jnp.transpose(held, tuple(reversed(range(bits))) + (bits, bits + 1))
+    pieces = {0: held.reshape(ranks * depth, width)}
+    bit = parts >> 1
+    while bit:
+        pieces.update({index ^ bit: swap(piece, "dp", bit) for index, piece in pieces.items()})
+        bit >>= 1
+    return [pieces[index] for index in range(parts)]
 
 
 def on_device(queries, key_maps, value_rows, gate_logits, mix_lambda, head_gain, out_weight):
@@ -126,14 +147,13 @@
     ranks = lax.axis_size("sp")
     items = seqs * heads // ranks
     width = gate_logits.shape[2]
+    pieces = gather_weight(out_weight)
     sent = jnp.stack([a.reshape(ranks, items, rows, cols) for a in (queries, key_maps, value_rows)], axis=2)
     got = lax.all_to_all(sent, "sp", split_axis=0, concat_axis=0, tiled=True)
     normed = attend(got, mix_lambda, head_gain)
     returned = lax.all_to_all(normed, "sp", split_axis=0, concat_axis=0, tiled=True)
-    weight = lax.all_gather(out_weight, "sp", axis=0, tiled=True)
-    weight = lax.all_gather(weight, "dp", axis=0, tiled=False)
     result = project(
-        returned.reshape(seqs, heads, rows, cols), gate_logits.reshape(rows * seqs, width), weight
+        returned.reshape(seqs, heads, rows, cols), gate_logits.reshape(rows * seqs, width), pieces
     )
     return result.reshape(rows, seqs, width)
 

time: 201 us -> 233 us (1.16)
  waiting for transfers between devices: 148 us -> 181 us
  between operations: 13.4 us -> 0.08 us
  starting transfers between devices: 7.37 us -> 20.4 us
    ppermute x0 -> x6, waiting for transfers between devices: none -> 157 us  [swap(): lax.ppermute(array, axis, [(i, i ^ bit) for i in range(lax.axis_size(axis...]
    all_to_all x1, waiting for transfers between devices: 69.6 us -> 0.01 us  [on_device(): got = lax.all_to_all(sent, 'sp', split_axis=0, concat_axis=0, tiled=True)]
    all_gather x2 -> x0, waiting for transfers between devices: 54 us -> none  [the longest x1 54 us: on_device(): weight = lax.all_gather(out_weight, 'sp', axis=0, tiled=True)]
    ppermute x0 -> x6, starting transfers between devices: none -> 6.45 us  [swap(): lax.ppermute(array, axis, [(i, i ^ bit) for i in range(lax.axis_size(axis...]
    all_to_all x1, starting transfers between devices: 3.7 us -> 7.44 us  [on_device(): got = lax.all_to_all(sent, 'sp', split_axis=0, concat_axis=0, tiled=True)]
    all_to_all x1, starting transfers between devices: 3.63 us -> 6.54 us  [on_device(): lax.all_to_all(normed, 'sp', split_axis=0, concat_axis=0, tiled=True)]
  transfers between devices with their start and end apart: 4 -> 8, of which waited for: 3 -> 5; matrix products, arithmetic and copies ran while one was open for 3% -> 1% of each run, Pallas kernels for 7% -> 6%
where the time goes in v2:
time: 233 us
  waiting for transfers between devices  181 us (78%)
  Pallas kernels  21.5 us (9%)
  starting transfers between devices  20.4 us (9%)
  local copies, waits for them, and re-layouts  5.58 us (2%)
  other arithmetic  4.45 us (2%)
    ppermute x6, waiting for transfers between devices, swap(): lax.ppermute(array, axis, [(i, i ^ bit) for i in range(lax.axis_size(axis...  157 us
    all_to_all x1, waiting for transfers between devices, on_device(): lax.all_to_all(normed, 'sp', split_axis=0, concat_axis=0, tiled=True)  24.3 us
    pallas_call x1, Pallas kernels, attend(): pl.pallas_call(attend_kernel, grid=(items,), out_shape=jax.ShapeDtypeStru...  13.5 us
    pallas_call x1, Pallas kernels, project(): pl.pallas_call(project_kernel, out_shape=jax.ShapeDtypeStruct((total, len...  7.93 us
    all_to_all x1, starting transfers between devices, on_device(): got = lax.all_to_all(sent, 'sp', split_axis=0, concat_axis=0, tiled=True)  7.44 us
    all_to_all x1, starting transfers between devices, on_device(): lax.all_to_all(normed, 'sp', split_axis=0, concat_axis=0, tiled=True)  6.54 us
    ppermute x6, starting transfers between devices, swap(): lax.ppermute(array, axis, [(i, i ^ bit) for i in range(lax.axis_size(axis...  6.45 us
  transfers between devices with their start and end apart: 8, of which 5 were waited for; matrix products, arithmetic and copies ran while one was open for 1% of the time, Pallas kernels for 6%

profile of v2, /device:TPU:0, one launch (start us, length us, event | category | flops | bytes accessed | tf_op | source)
XLA Modules:
  0.0 233.1 jit_solution(1559240962062711778)
XLA Ops:
  0.0 3.9 %pad_maximum_fusion = bf16[8,8,3,64,128]{4,3,2,1,0:T(8,128)(2,1)} fusion(bf16[8,8,1,64,128]{4,3,2,1,0:T(8,128)(2,1)} %bitcast.26, bf16[8,8,1,64,128]{4,3,2,1,0:T(8,128)(2,1)} %bitcast.27, bf16[8,8,1,64,128]{4,3,2,1,0:T(8,128)(2,1)} %bitcast.28), kind=kLoop, calls=%fused_computation | loop fusion | flops 3145728 | bytes 6291456 | tf_op jit(solution)/shard_map/stack | solution.py:151
  3.9 0.0 copy-start.2
  3.9 7.4 %all-to-all-start = ((bf16[8,8,3,64,128]{4,3,2,1,0:T(8,128)(2,1)}), bf16[8,8,3,64,128]{4,3,2,1,0:T(8,128)(2,1)}, u32[]{:S(2)}, u32[]{:S(2)}) async-start(bf16[8,8,3,64,128]{4,3,2,1,0:T(8,128)(2,1)} %pad_maximum_fusion), calls=%async_computation | async-start | bytes 6291456 | tf_op jit(solution)/shard_map/all_to_all | solution.py:152
  11.3 0.0 copy-done.2
  11.3 2.9 %collective-permute-start = (bf16[256,512]{1,0:T(8,128)(2,1)S(1)}, bf16[256,512]{1,0:T(8,128)(2,1)S(1)}, u32[]{:S(2)}, u32[]{:S(2)}) collective-permute-start(bf16[256,512]{1,0:T(8,128)(2,1)S(1)} %copy-done.2), channel_id=1, source_target_pairs={{0,16},{4,20},{8,24},{12,28},{16,0},{20,4},{24,8},{28,12},{1,17},{... | collective-permute-start | bytes 786440 | tf_op jit(solution)/shard_map/ppermute | solution.py:123
  14.2 79.0 %collective-permute-done = bf16[256,512]{1,0:T(8,128)(2,1)S(1)} collective-permute-done((bf16[256,512]{1,0:T(8,128)(2,1)S(1)}, bf16[256,512]{1,0:T(8,128)(2,1)S(1)}, u32[]{:S(2)}, u32[]{:S(2)}) %collective-permute-start) | collective-permute-done | bytes 262176 | tf_op jit(solution)/shard_map/ppermute | solution.py:123
  93.3 0.1 pad_maximum_fusion.2
  93.3 0.1 collective-permute-start.1
  93.4 12.6 %collective-permute-done.1 = bf16[2,256,512]{2,1,0:T(8,128)(2,1)S(1)} collective-permute-done((bf16[2,256,512]{2,1,0:T(8,128)(2,1)S(1)}, bf16[2,256,512]{2,1,0:T(8,128)(2,1)S(1)}, u32[]{:S(2)}, u32[]{:S(2)}) %collective-permute-start.1) | collective-permute-done | bytes 524320 | tf_op jit(solution)/shard_map/ppermute | solution.py:123
  106.0 0.1 select_bitcast_fusion.3
  106.1 0.1 pad_maximum_fusion.1
  106.2 1.9 collective-permute-start.2
  108.1 21.6 %collective-permute-done.2 = bf16[2,2,256,512]{3,2,1,0:T(8,128)(2,1)S(1)} collective-permute-done((bf16[2,2,256,512]{3,2,1,0:T(8,128)(2,1)S(1)}, bf16[2,2,256,512]{3,2,1,0:T(8,128)(2,1)S(1)}, u32[]{:S(2)}, u32[]{:S(2)}) %collective-permute-start.2) | collective-permute-done | bytes 1048608 | tf_op jit(solution)/shard_map/ppermute | solution.py:123
  129.6 0.1 select_bitcast_fusion.1
  129.8 0.2 maximum_bitcast_fusion
  130.0 0.2 copy.8
  130.2 0.0 copy-start
  130.2 1.6 collective-permute-start.4
  131.8 0.0 collective-permute-start.3
  131.8 43.6 %collective-permute-done.4.refs_2_ = bf16[2048,512]{1,0:T(8,128)(2,1)} collective-permute-done((bf16[2048,512]{1,0:T(8,128)(2,1)S(1)}, bf16[2048,512]{1,0:T(8,128)(2,1)}, u32[]{:S(2)}, u32[]{:S(2)}) %collective-permute-start.4) | collective-permute-done | bytes 2097184 | tf_op jit(solution)/shard_map/ppermute | solution.py:123
  175.4 0.0 collective-permute-start.5
  175.4 0.0 all-to-all-done.got_ref
  175.4 13.5 %attend.1 = bf16[8,8,64,128]{3,2,1,0:T(8,128)(2,1)} custom-call(s32[1]{0:T(128)} %bitcast.1.place_ref, f32[16]{0:T(128)} %lam_ref.1, f32[1,128]{1,0:T(1,128)} %bitcast.29, bf16[8,8,3,64,128]{4,3,2,1,0:T(8,128)(2,1)} %all-to-all-done.got_ref), custom_call_target="tpu_custom_call" | custom-call | flops 6000000000 | bytes 4000000 | tf_op jit(solution)/shard_map/attend/pallas_call | solution.py:69
  189.0 0.0 copy-done
  189.0 6.5 %all-to-all-start.1 = ((bf16[8,8,64,128]{3,2,1,0:T(8,128)(2,1)}), bf16[8,8,64,128]{3,2,1,0:T(8,128)(2,1)S(1)}, u32[]{:S(2)}, u32[]{:S(2)}) async-start(bf16[8,8,64,128]{3,2,1,0:T(8,128)(2,1)} %attend.1), calls=%async_computation.1 | async-start | bytes 2097152 | tf_op jit(solution)/shard_map/all_to_all | solution.py:154
  195.5 2.1 reshape.13.gate_ref
  197.7 0.0 collective-permute-done.3.refs_1_
  197.7 0.0 collective-permute-done.5.refs_3_
  197.7 24.3 %all-to-all-done.1 = bf16[8,8,64,128]{3,2,1,0:T(8,128)(2,1)S(1)} async-done(((bf16[8,8,64,128]{3,2,1,0:T(8,128)(2,1)}), bf16[8,8,64,128]{3,2,1,0:T(8,128)(2,1)S(1)}, u32[]{:S(2)}, u32[]{:S(2)}) %all-to-all-start.1) | async-done | bytes 1048608 | tf_op jit(solution)/shard_map/all_to_all | solution.py:154
  221.9 0.0 copy-start.1
  221.9 1.0 copy-done.1
  222.9 7.9 %project.1 = bf16[256,2048]{1,0:T(8,128)(2,1)} custom-call(s32[1]{0:T(128)} %bitcast.place_ref, bf16[4,16,64,128]{3,2,1,0:T(8,128)(2,1)} %bitcast.25, bf16[256,2048]{1,0:T(8,128)(2,1)} %reshape.13.gate_ref, bf16[2048,512]{1,0:T(8,128)(2,1)} %bitcast.24, bf16[2048,512]{1,0:T(8,128)(2,1)} %collective-permute-done.3.refs_1_, ...), custom_call_target="tpu_custom_call" | custom-call | flops 2000000000 | bytes 10000000 | tf_op jit(solution)/shard_map/project/pallas_call | solution.py:111
  230.8 2.2 reshape.15
  (1 shorter events, 0.0 us)
Async XLA Ops:
  3.9 7.4 %copy-start.2 = (bf16[256,512]{1,0:T(8,128)(2,1)S(1)}, bf16[256,512]{1,0:T(8,128)(2,1)}, u32[]{:S(2)}) copy-start(bf16[256,512]{1,0:T(8,128)(2,1)} %param.13) | copy-start | bytes 786436
  3.9 171.6 %all-to-all-start = ((bf16[8,8,3,64,128]{4,3,2,1,0:T(8,128)(2,1)}), bf16[8,8,3,64,128]{4,3,2,1,0:T(8,128)(2,1)}, u32[]{:S(2)}, u32[]{:S(2)}) async-start(bf16[8,8,3,64,128]{4,3,2,1,0:T(8,128)(2,1)} %pad_maximum_fusion), calls=%async_computation | async-start | bytes 6291456 | tf_op jit(solution)/shard_map/all_to_all | solution.py:152
  11.3 81.9 %collective-permute-start = (bf16[256,512]{1,0:T(8,128)(2,1)S(1)}, bf16[256,512]{1,0:T(8,128)(2,1)S(1)}, u32[]{:S(2)}, u32[]{:S(2)}) collective-permute-start(bf16[256,512]{1,0:T(8,128)(2,1)S(1)} %copy-done.2), channel_id=1, source_target_pairs={{0,16},{4,20},{8,24},{12,28},{16,0},{20,4},{24,8},{28,12},{1,17},{... | collective-permute-start | bytes 786440 | tf_op jit(solution)/shard_map/ppermute | solution.py:123
  93.3 12.6 %collective-permute-start.1 = (bf16[2,256,512]{2,1,0:T(8,128)(2,1)S(1)}, bf16[2,256,512]{2,1,0:T(8,128)(2,1)S(1)}, u32[]{:S(2)}, u32[]{:S(2)}) collective-permute-start(bf16[2,256,512]{2,1,0:T(8,128)(2,1)S(1)} %pad_maximum_fusion.2), channel_id=1, source_target_pairs={{0,8},{4,12},{8,0},{12,4},{16,24},{20,28},{24,16},{28,20},{1,9},{5... | collective-permute-start | bytes 1572872 | tf_op jit(solution)/shard_map/ppermute | solution.py:123
  106.2 23.5 %collective-permute-start.2 = (bf16[2,2,256,512]{3,2,1,0:T(8,128)(2,1)S(1)}, bf16[2,2,256,512]{3,2,1,0:T(8,128)(2,1)S(1)}, u32[]{:S(2)}, u32[]{:S(2)}) collective-permute-start(bf16[2,2,256,512]{3,2,1,0:T(8,128)(2,1)S(1)} %pad_maximum_fusion.1), channel_id=1, source_target_pairs={{0,4},{4,0},{8,12},{12,8},{16,20},{20,16},{24,28},{28,24},{1,5},{5... | collective-permute-start | bytes 3145736 | tf_op jit(solution)/shard_map/ppermute | solution.py:123
  130.2 58.8 %copy-start = (bf16[2,2,2,256,512]{4,3,2,1,0:T(8,128)(2,1)}, bf16[2,2,2,256,512]{4,3,2,1,0:T(8,128)(2,1)S(1)}, u32[]{:S(2)}) copy-start(bf16[2,2,2,256,512]{4,3,2,1,0:T(8,128)(2,1)S(1)} %copy.8) | copy-start | bytes 6291460
  130.2 45.2 %collective-permute-start.4 = (bf16[2048,512]{1,0:T(8,128)(2,1)S(1)}, bf16[2048,512]{1,0:T(8,128)(2,1)}, u32[]{:S(2)}, u32[]{:S(2)}) collective-permute-start(bf16[2048,512]{1,0:T(8,128)(2,1)S(1)} %bitcast.22), channel_id=1, source_target_pairs={{0,2},{1,3},{2,0},{3,1},{4,6},{5,7},{6,4},{7,5},{8,10},{9,11},{10,... | collective-permute-start | bytes 6291464 | tf_op jit(solution)/shard_map/ppermute | solution.py:123
  131.8 65.9 %collective-permute-start.3 = (bf16[2048,512]{1,0:T(8,128)(2,1)S(1)}, bf16[2048,512]{1,0:T(8,128)(2,1)}, u32[]{:S(2)}, u32[]{:S(2)}) collective-permute-start(bf16[2048,512]{1,0:T(8,128)(2,1)S(1)} %bitcast.23), channel_id=1, source_target_pairs={{0,1},{1,0},{2,3},{3,2},{4,5},{5,4},{6,7},{7,6},{8,9},{9,8},{10,11... | collective-permute-start | bytes 6291464 | tf_op jit(solution)/shard_map/ppermute | solution.py:123
  175.4 22.2 %collective-permute-start.5 = (bf16[2048,512]{1,0:T(8,128)(2,1)}, bf16[2048,512]{1,0:T(8,128)(2,1)}, u32[]{:S(2)}, u32[]{:S(2)}) collective-permute-start(bf16[2048,512]{1,0:T(8,128)(2,1)} %collective-permute-done.4.refs_2_), channel_id=1, source_target_pairs={{0,1},{1,0},{2,3},{3,2},{4,5},{5,4},{6,7},{7,6},{8,9},{9,8},{10,11... | collective-permute-start | bytes 6291464 | tf_op jit(solution)/shard_map/ppermute | solution.py:123
  189.0 33.0 %all-to-all-start.1 = ((bf16[8,8,64,128]{3,2,1,0:T(8,128)(2,1)}), bf16[8,8,64,128]{3,2,1,0:T(8,128)(2,1)S(1)}, u32[]{:S(2)}, u32[]{:S(2)}) async-start(bf16[8,8,64,128]{3,2,1,0:T(8,128)(2,1)} %attend.1), calls=%async_computation.1 | async-start | bytes 2097152 | tf_op jit(solution)/shard_map/all_to_all | solution.py:154
  221.9 1.0 copy-start.1
